TPU v7x, 32 devices: a whole 2x2x4 slice. The times are simulated.
32 devices in a mesh: dp: 4 (over y, x), kv: 4 (over z), tp: 2 (over core).
Axes of the slice: x: 2, y: 2, z: 4, core: 2. Of those that a mesh axis runs over, the one named last changes fastest.
Arguments:
- tokens: bfloat16 [128, 2048], P('dp', ('kv', 'tp')), may hold values from -60 to 60
- first_norm_gain: float32 [2048], replicated, may hold values from 0.1 to 1.9
- first_gate_weight: bfloat16 [2048, 5632], P(None, ('kv', 'tp')), may hold values from -0.125 to 0.125
- first_up_weight: bfloat16 [2048, 5632], P(None, ('kv', 'tp')), may hold values from -0.125 to 0.125
- first_down_weight: bfloat16 [5632, 2048], P(('kv', 'tp')), may hold values from -0.109375 to 0.109375
- mixer_norm_gain: float32 [2048], replicated, may hold values from 0.1 to 1.9
- query_weight: bfloat16 [2048, 1024], P('kv', 'tp'), may hold values from -0.125 to 0.125
- key_weight: bfloat16 [2048, 1024], P('kv', 'tp'), may hold values from -0.125 to 0.125
- value_weight: bfloat16 [2048, 1024], P('kv', 'tp'), may hold values from -0.125 to 0.125
- output_gate_weight: bfloat16 [2048, 1024], P('kv', 'tp'), may hold values from -0.125 to 0.125
- strength_weight: bfloat16 [2048, 8], replicated, may hold values from -0.125 to 0.125
- decay_weight: bfloat16 [2048, 8], replicated, may hold values from -0.125 to 0.125
- head_decay_log: float32 [8], replicated, may hold values from 0 to 2.77
- decay_input_bias: float32 [8], replicated, may hold values from -4 to 0
- decay_extra_log: float32 [128, 8], P(('dp', 'kv'), 'tp'), may hold values from -0.7 to 0
- head_norm_gain: float32 [128], replicated, may hold values from 0.1 to 1.9
- state: float32 [128, 8, 128, 128], P(('dp', 'kv'), 'tp'), may hold values from -0.6 to 0.6
- mixer_output_weight: bfloat16 [1024, 2048], P('tp', 'kv'), may hold values from -0.1875 to 0.1875
- second_norm_gain: float32 [2048], replicated, may hold values from 0.1 to 1.9
- second_gate_weight: bfloat16 [2048, 5632], P(None, ('kv', 'tp')), may hold values from -0.125 to 0.125
- second_up_weight: bfloat16 [2048, 5632], P(None, ('kv', 'tp')), may hold values from -0.125 to 0.125
- second_down_weight: bfloat16 [5632, 2048], P(('kv', 'tp')), may hold values from -0.109375 to 0.109375
Outputs:
- layer_out: bfloat16 [128, 2048], P('dp', ('kv', 'tp'))
- new_state: float32 [128, 8, 128, 128], P(('dp', 'kv'), 'tp')
All inputs are finite; a program needn't handle non-finite values.
Results may differ from a plain program's by a relative error of at most 0.014.
Values may be sent and summed in bfloat16 or wider, within the bound.
A program may use at most 64 MiB of HBM per device.

v0:
```python
import jax
import jax.numpy as jnp
from jax import lax
from jax.sharding import PartitionSpec as P

EPS = 1e-06


def row_scale(values):
    return lax.rsqrt(jnp.mean(values * values, axis=-1, keepdims=True) + EPS)


def unit_rows(values):
    return values * lax.rsqrt(jnp.sum(values * values, axis=-1, keepdims=True) + EPS)


def block_terms(row_data, gain_vec, w_gate, w_up, w_down):
    rows32 = row_data.astype(jnp.float32)
    normed = (rows32 * row_scale(rows32) * gain_vec).astype(jnp.bfloat16)
    gate_pre = jnp.dot(normed, w_gate, preferred_element_type=jnp.float32)
    upward = jnp.dot(normed, w_up, preferred_element_type=jnp.float32)
    hidden = (jax.nn.silu(gate_pre) * upward).astype(jnp.bfloat16)
    return jnp.dot(hidden, w_down, preferred_element_type=jnp.float32)


def delta_step(
    query_vec, key_vec, value_vec, gate_vals, beta_gate, head_decay_rate, state, head_norm_gain
):
    recalled = jnp.einsum("shd,shde->she", key_vec, state, precision=lax.Precision.HIGHEST)
    correction = beta_gate[..., None] * (value_vec - head_decay_rate[..., None] * recalled)
    new_state = (
        head_decay_rate[..., None, None] * state + key_vec[..., :, None] * correction[..., None, :]
    )
    read_out = jnp.einsum("shd,shde->she", query_vec, new_state, precision=lax.Precision.HIGHEST)
    normed = read_out * row_scale(read_out) * head_norm_gain
    return (normed * jax.nn.silu(gate_vals), new_state)


def shards(
    tokens,
    first_norm_gain,
    first_gate_weight,
    first_up_weight,
    first_down_weight,
    mixer_norm_gain,
    query_weight,
    key_weight,
    value_weight,
    output_gate_weight,
    strength_weight,
    decay_weight,
    head_decay_log,
    decay_input_bias,
    decay_extra_log,
    head_norm_gain,
    state,
    mixer_output_weight,
    second_norm_gain,
    second_gate_weight,
    second_up_weight,
    second_down_weight,
):
    batch_rows, columns = tokens.shape
    kv_index = lax.axis_index("kv")
    tp_index = lax.axis_index("tp")
    own_block = kv_index * lax.axis_size("tp") + tp_index
    seq_dev, heads_dev, head_size = (state.shape[0], state.shape[1], state.shape[2])
    kv_width = query_weight.shape[0]
    head_cols = heads_dev * head_size
    model_width = mixer_norm_gain.shape[0]
    rows_all = lax.all_gather(tokens, ("kv", "tp"), axis=1, tiled=True)
    ffn_terms = block_terms(
        rows_all, first_norm_gain, first_gate_weight, first_up_weight, first_down_weight
    )
    share_sum = lax.psum_scatter(
        ffn_terms.astype(jnp.bfloat16), ("kv", "tp"), scatter_dimension=1, tiled=True
    ).astype(jnp.float32)
    first_rows = (tokens.astype(jnp.float32) + 0.5 * share_sum).astype(jnp.bfloat16)
    first32 = first_rows.astype(jnp.float32)
    kv_block = lax.all_gather(first_rows, "tp", axis=1, tiled=True)
    own_gain = lax.dynamic_slice_in_dim(mixer_norm_gain, own_block * columns, columns)
    own_scaled = (first32 * own_gain).astype(jnp.bfloat16)
    beta_rows = lax.dynamic_slice_in_dim(strength_weight, own_block * columns, columns, 0)
    decay_rows = lax.dynamic_slice_in_dim(decay_weight, own_block * columns, columns, 0)
    squares, beta_pre, decay_logits = lax.psum(
        (
            jnp.sum(first32 * first32, axis=1),
            jnp.dot(own_scaled, beta_rows, preferred_element_type=jnp.float32),
            jnp.dot(own_scaled, decay_rows, preferred_element_type=jnp.float32),
        ),
        ("kv", "tp"),
    )
    row_factor = lax.rsqrt(squares / model_width + EPS)
    block_gain = lax.dynamic_slice_in_dim(mixer_norm_gain, kv_index * kv_width, kv_width)
    block_scaled = (kv_block.astype(jnp.float32) * block_gain).astype(jnp.bfloat16)
    projected = lax.psum_scatter(
        jnp.concatenate(
            [
                jnp.dot(block_scaled, weight, preferred_element_type=jnp.float32)
                for weight in (query_weight, key_weight, value_weight, output_gate_weight)
            ],
            axis=1,
        ).astype(jnp.bfloat16),
        "kv",
        scatter_dimension=0,
        tiled=True,
    ).astype(jnp.float32)
    own_rows = kv_index * seq_dev
    own_factor = lax.dynamic_slice_in_dim(row_factor, own_rows, seq_dev)[:, None]
    projected = projected * own_factor

    def split_heads(role_index):
        return projected[:, role_index * head_cols : (role_index + 1) * head_cols].reshape(
            seq_dev, heads_dev, head_size
        )

    query_vec = unit_rows(jax.nn.silu(split_heads(0))) * head_size ** (-0.5)
    key_vec = unit_rows(jax.nn.silu(split_heads(1)))
    value_vec = jax.nn.silu(split_heads(2))
    gate_vals = split_heads(3)
    head_start = tp_index * heads_dev

    def local_gate_values(values):
        own_seqs = lax.dynamic_slice_in_dim(values, own_rows, seq_dev, 0)
        return lax.dynamic_slice_in_dim(own_seqs, head_start, heads_dev, 1) * own_factor

    beta_gate = jax.nn.sigmoid(local_gate_values(beta_pre))
    decay_log_term = lax.dynamic_slice_in_dim(head_decay_log, head_start, heads_dev)
    decay_offset_term = lax.dynamic_slice_in_dim(decay_input_bias, head_start, heads_dev)
    head_decay_rate = jnp.exp(
        decay_extra_log
        - jnp.exp(decay_log_term)
        * jax.nn.softplus(local_gate_values(decay_logits) + decay_offset_term)
    )
    heads_f32, new_state = delta_step(
        query_vec, key_vec, value_vec, gate_vals, beta_gate, head_decay_rate, state, head_norm_gain
    )
    heads_out = heads_f32.reshape(seq_dev, head_cols).astype(jnp.bfloat16)
    mixer_terms = jnp.dot(
        lax.all_gather(heads_out, "kv", axis=0, tiled=True),
        mixer_output_weight,
        preferred_element_type=jnp.float32,
    )
    mixer_sum = lax.psum_scatter(
        mixer_terms.astype(jnp.bfloat16), "tp", scatter_dimension=1, tiled=True
    ).astype(jnp.float32)
    second_rows = (first32 + mixer_sum).astype(jnp.bfloat16)
    rows_last = lax.all_gather(second_rows, ("kv", "tp"), axis=1, tiled=True)
    last_terms = block_terms(
        rows_last, second_norm_gain, second_gate_weight, second_up_weight, second_down_weight
    )
    last_sum = lax.psum_scatter(
        last_terms.astype(jnp.bfloat16), ("kv", "tp"), scatter_dimension=1, tiled=True
    ).astype(jnp.float32)
    layer_out = (second_rows.astype(jnp.float32) + 0.5 * last_sum).astype(jnp.bfloat16)
    return (layer_out, new_state)


def solution(mesh):
    placed = (
        P("dp", ("kv", "tp")),
        P(),
        P(None, ("kv", "tp")),
        P(None, ("kv", "tp")),
        P(("kv", "tp"), None),
        P(),
        P("kv", "tp"),
        P("kv", "tp"),
        P("kv", "tp"),
        P("kv", "tp"),
        P(),
        P(),
        P(),
        P(),
        P(("dp", "kv"), "tp"),
        P(),
        P(("dp", "kv"), "tp", None, None),
        P("tp", "kv"),
        P(),
        P(None, ("kv", "tp")),
        P(None, ("kv", "tp")),
        P(("kv", "tp"), None),
    )
    return jax.shard_map(
        shards,
        mesh=mesh,
        in_specs=placed,
        out_specs=(P("dp", ("kv", "tp")), P(("dp", "kv"), "tp", None, None)),
        check_vma=False,
    )
```

profile of v0, /device:TPU:0, one launch (start us, length us, event | category | flops | bytes accessed | tf_op | source)
XLA Modules:
  0.0 181.2 jit_solution(4792796293112144642)
XLA Ops:
  7.2 16.1 %all_gather.12 = bf16[32,2048]{1,0:T(8,128)(2,1)S(1)} all-gather(bf16[32,256]{1,0:T(8,128)(2,1)} %param.22), channel_id=1, replica_groups=mesh['dp'=4,'kv'=4,'tp'=2] {'kv','tp'}, dimensions={1}, use_global_device_ids=true | all-gather | bytes 147456 | tf_op jit(solution)/shard_map/all_gather | solution.py:71
  24.0 3.4 %fusion.26 = f32[32,704]{1,0:T(8,128)} fusion(bf16[2048,704]{0,1:T(8,128)(2,1)} %param.24, bf16[32,2048]{1,0:T(8,128)(2,1)S(1)} %all_gather.12, f32[2048]{0:T(1024)} %param.23, f32[32]{0:T(128)S(1)} %add_rsqrt_fusion.5), kind=kOutput, calls=%fused_computation.41 | convolution fusion | flops 92536832 | bytes 3113088 | tf_op jit(solution)/shard_map/dot_general | solution.py:20
  27.4 4.3 %convolution_convert_fusion.1 = bf16[32,2048]{1,0:T(8,128)(2,1)} fusion(bf16[704,2048]{1,0:T(8,128)(2,1)S(1)} %copy-done, bf16[2048,704]{0,1:T(8,128)(2,1)} %param.25, f32[32,704]{1,0:T(8,128)} %fusion.26, bf16[32,2048]{1,0:T(8,128)(2,1)S(1)} %all_gather.12, f32[2048]{0:T(1024)} %param.23, f32[32]{0:T(128)} %copy-done.8), kind=kOutput, calls=%fused_computation.1 | convolution fusion | flops 185012224 | bytes 6127744 | tf_op jit(solution)/shard_map/dot_general | solution.py:23
  34.8 28.7 %reduce-scatter.5.cloned.1.call-done = bf16[32,256]{1,0:T(8,128)(2,1)} async-done(((bf16[32,2048]{1,0:T(8,128)(2,1)}), bf16[32,256]{1,0:T(8,128)(2,1)}) %reduce-scatter.5.cloned.1.call-update) | async-done | bytes 16400 | tf_op jit(solution)/shard_map/reduce_scatter | solution.py:75
  63.5 0.8 fusion.28
  64.3 1.8 %all_gather.13 = bf16[32,512]{1,0:T(8,128)(2,1)S(1)} all-gather(bf16[32,256]{1,0:T(8,128)(2,1)S(1)} %get-tuple-element.8), channel_id=1, replica_groups=mesh['dp'=4,'kv'=4,'tp'=2] {'tp'}, dimensions={1}, use_global_device_ids=true | all-gather | bytes 49152 | tf_op jit(solution)/shard_map/all_gather | solution.py:80
  66.2 0.8 fusion.43
  67.0 0.8 fusion.41
  68.0 1.2 convolution_convert_fusion.4
  69.2 1.2 convolution_convert_fusion.3
  70.5 1.3 convolution_convert_fusion.6
  72.5 14.4 %all-reduce = (f32[32]{0:T(128)S(1)}, f32[32,8]{0,1:T(8,128)S(1)}, f32[32,8]{0,1:T(8,128)S(1)}) all-reduce(f32[32]{0:T(128)S(1)} %get-tuple-element.7, f32[32,8]{0,1:T(8,128)S(1)} %fusion.43, f32[32,8]{0,1:T(8,128)S(1)} %fusion.41), channel_id=1, replica_groups=mesh['dp'=4,'kv'=4,'tp'=2] {'kv','tp'}, use_global_device_ids=true, to_apply=%region_4.5 | all-reduce | flops 544 | bytes 4352 | tf_op jit(solution)/shard_map/psum | solution.py:85
  87.1 3.0 %reduce-scatter.7.cloned.1.call-done = bf16[8,2048]{1,0:T(8,128)(2,1)} async-done(((bf16[32,2048]{1,0:T(8,128)(2,1)}), bf16[8,2048]{1,0:T(8,128)(2,1)}) %reduce-scatter.7.cloned.1.call-update) | async-done | bytes 32784 | tf_op jit(solution)/shard_map/reduce_scatter | solution.py:96
  90.1 1.0 convert_multiply_fusion.4
  91.4 3.4 %fusion.39 = f32[8,4,1,128]{3,2,1,0:T(1,128)S(1)} fusion(f32[8,4,128,128]{3,2,1,0:T(8,128)} %param.38, f32[8,4,128,1]{2,0,1,3:T(8,128)S(1)} %fusion.69), kind=kOutput, calls=%fused_computation.62 | convolution fusion | flops 6291456 | bytes 2129920 | tf_op jit(solution)/shard_map/shd,shde->she/dot_general | solution.py:29
  95.7 1.3 copy-done.2
  97.0 1.9 %fusion.37 = f32[8,4,1,128]{3,2,1,0:T(1,128)S(1)} fusion(f32[8,4,128,128]{3,2,1,0:T(8,128)S(1)} %multiply_add_fusion, f32[8,4,128,1]{2,0,1,3:T(8,128)S(1)} %get-tuple-element.9), kind=kOutput, calls=%fused_computation.60 | convolution fusion | flops 6291456 | bytes 2129920 | tf_op jit(solution)/shard_map/shd,shde->she/dot_general | solution.py:34
  99.1 13.1 %all_gather.14 = bf16[32,512]{1,0:T(8,128)(2,1)S(1)} all-gather(bf16[8,512]{1,0:T(8,128)(2,1)S(1)} %fusion.45), channel_id=1, replica_groups=mesh['dp'=4,'kv'=4,'tp'=2] {'kv'}, dimensions={0}, use_global_device_ids=true | all-gather | bytes 40960 | tf_op jit(solution)/shard_map/all_gather | solution.py:140
  113.1 5.8 %reduce-scatter.9.cloned.1.call-done = bf16[32,256]{1,0:T(8,128)(2,1)} async-done(((bf16[32,512]{1,0:T(8,128)(2,1)}), bf16[32,256]{1,0:T(8,128)(2,1)}) %reduce-scatter.9.cloned.1.call-update) | async-done | bytes 16400 | tf_op jit(solution)/shard_map/reduce_scatter | solution.py:144
  119.6 14.3 %all_gather.15 = bf16[32,2048]{1,0:T(8,128)(2,1)S(1)} all-gather(bf16[32,256]{1,0:T(8,128)(2,1)S(1)} %fusion.30), channel_id=1, replica_groups=mesh['dp'=4,'kv'=4,'tp'=2] {'kv','tp'}, dimensions={1}, use_global_device_ids=true | all-gather | bytes 147456 | tf_op jit(solution)/shard_map/all_gather | solution.py:148
  134.0 2.7 %fusion.22 = f32[32,704]{1,0:T(8,128)S(1)} fusion(bf16[2048,704]{0,1:T(8,128)(2,1)} %param.41, bf16[32,2048]{1,0:T(8,128)(2,1)S(1)} %all_gather.15, f32[2048]{0:T(1024)S(1)} %copy-done.6, f32[32]{0:T(128)S(1)} %add_rsqrt_fusion.3), kind=kOutput, calls=%fused_computation.40 | convolution fusion | flops 92536832 | bytes 3113088 | tf_op jit(solution)/shard_map/dot_general | solution.py:20
  136.7 5.1 %convolution_convert_fusion = bf16[32,2048]{1,0:T(8,128)(2,1)} fusion(bf16[704,2048]{1,0:T(8,128)(2,1)} %param.43, bf16[2048,704]{0,1:T(8,128)(2,1)} %param.42, f32[32,704]{1,0:T(8,128)S(1)} %fusion.22, bf16[32,2048]{1,0:T(8,128)(2,1)S(1)} %all_gather.15, f32[2048]{0:T(1024)S(1)} %copy-done.6, f32[32]{0:T(128)S(1)} %add_rsqrt_fusion.3), kind=kOutput, calls=%fused_computation | convolution fusion | flops 185012224 | bytes 6127744 | tf_op jit(solution)/shard_map/dot_general | solution.py:23
  141.9 31.5 %reduce-scatter.11.cloned.1.call-done = bf16[32,256]{1,0:T(8,128)(2,1)} async-done(((bf16[32,2048]{1,0:T(8,128)(2,1)}), bf16[32,256]{1,0:T(8,128)(2,1)}) %reduce-scatter.11.cloned.1.call-update) | async-done | bytes 16400 | tf_op jit(solution)/shard_map/reduce_scatter | solution.py:152
  173.4 1.3 add_convert_fusion
  (54 shorter events, 8.0 us)
Async XLA Ops:
  7.2 20.2 %copy-start = (bf16[704,2048]{1,0:T(8,128)(2,1)S(1)}, bf16[704,2048]{1,0:T(8,128)(2,1)}, u32[]{:S(2)}) copy-start(bf16[704,2048]{1,0:T(8,128)(2,1)} %param.26) | copy-start | bytes 8650756
  7.2 56.3 %reduce-scatter.5.cloned.1.call-start = ((), (), s32[]{:S(2)}) async-start(), calls=%async_computation.4 | async-start | bytes 147456 | tf_op jit(solution)/shard_map/reduce_scatter | solution.py:75
  23.5 0.5 copy-start.8
  27.4 36.2 %copy-start.5 = (bf16[32,256]{1,0:T(8,128)(2,1)S(1)}, bf16[32,256]{1,0:T(8,128)(2,1)}, u32[]{:S(2)}) copy-start(bf16[32,256]{1,0:T(8,128)(2,1)} %param.22) | copy-start | bytes 49156
  27.4 40.4 %copy-start.3 = (bf16[512,512]{1,0:T(8,128)(2,1)S(1)}, bf16[512,512]{1,0:T(8,128)(2,1)}, u32[]{:S(2)}) copy-start(bf16[512,512]{1,0:T(8,128)(2,1)} %param.29) | copy-start | bytes 1572868
  31.7 55.2 %copy-start.7 = (f32[8,4]{0,1:T(4,128)S(1)}, f32[8,4]{0,1:T(4,128)}, u32[]{:S(2)}) copy-start(f32[8,4]{0,1:T(4,128)} %param.36) | copy-start | bytes 388
  31.7 58.4 %reduce-scatter.7.cloned.1.call-start = ((), (), s32[]{:S(2)}) async-start(), calls=%async_computation.5 | async-start | bytes 163840 | tf_op jit(solution)/shard_map/reduce_scatter | solution.py:96
  72.4 46.4 %reduce-scatter.9.cloned.1.call-start = ((), (), s32[]{:S(2)}) async-start(), calls=%async_computation.6 | async-start | bytes 49152 | tf_op jit(solution)/shard_map/reduce_scatter | solution.py:144
  90.1 4.8 %copy-start.1 = (f32[8,4,128,128]{3,2,1,0:T(8,128)S(1)}, f32[8,4,128,128]{3,2,1,0:T(8,128)}, u32[]{:S(2)}) copy-start(f32[8,4,128,128]{3,2,1,0:T(8,128)} %param.38) | copy-start | bytes 6291460
  94.9 4.1 %copy-start.9 = (f32[128]{0:T(128)S(1)}, f32[128]{0:T(128)}, u32[]{:S(2)}) copy-start(f32[128]{0:T(128)} %param.37) | copy-start | bytes 1540
  94.9 17.3 %copy-start.4 = (bf16[512,512]{1,0:T(8,128)(2,1)S(1)}, bf16[512,512]{1,0:T(8,128)(2,1)}, u32[]{:S(2)}) copy-start(bf16[512,512]{1,0:T(8,128)(2,1)} %param.39) | copy-start | bytes 1572868
  94.9 39.1 %copy-start.6 = (f32[2048]{0:T(1024)S(1)}, f32[2048]{0:T(1024)}, u32[]{:S(2)}) copy-start(f32[2048]{0:T(1024)} %param.40) | copy-start | bytes 24580
  95.7 1.3 copy-start.2
  113.0 60.3 %reduce-scatter.11.cloned.1.call-start = ((), (), s32[]{:S(2)}) async-start(), calls=%async_computation.7 | async-start | bytes 147456 | tf_op jit(solution)/shard_map/reduce_scatter | solution.py:152
Sparse Core Ops, SparseCore 0:
  31.8 31.6 reduce-scatter.4
  72.5 17.5 reduce-scatter.6
  113.2 5.6 reduce-scatter.8
  142.0 31.3 reduce-scatter.10
where the time goes:
time: 182 us; the launch traced here: 181 us
  waiting for transfers between devices  69.1 us (38%)
  blocking collectives  59.7 us (33%)
  matrix products  27.2 us (15%)
  between operations  13.9 us (8%)
  other arithmetic  6.18 us (3%)
  local copies, waits for them, and re-layouts  5.02 us (3%)
    reduce_scatter x1, waiting for transfers between devices, shards(): lax.psum_scatter(last_terms.astype(jnp.bfloat16), ('kv', 'tp'), scatter_d...  31.5 us
    reduce_scatter x1, waiting for transfers between devices, shards(): lax.psum_scatter(ffn_terms.astype(jnp.bfloat16), ('kv', 'tp'), scatter_di...  28.7 us
    all_gather x1, blocking collectives, shards(): rows_all = lax.all_gather(tokens, ('kv', 'tp'), axis=1, tiled=True)  16.1 us
    psum x1, blocking collectives, shards(): lax.psum((jnp.sum(first32 * first32, axis=1), jnp.dot(own_scaled, beta_ro...  14.4 us
    all_gather x1, blocking collectives, shards(): rows_last = lax.all_gather(second_rows, ('kv', 'tp'), axis=1, tiled=True)  14.3 us
    all_gather x1, blocking collectives, shards(): lax.all_gather(heads_out, 'kv', axis=0, tiled=True)  13.1 us
    dot_general x2, matrix products, block_terms(): return jnp.dot(hidden, w_down, preferred_element_type=jnp.float32)  9.45 us
    dot_general x2, matrix products, block_terms(): gate_pre = jnp.dot(normed, w_gate, preferred_element_type=jnp.float32)  6.1 us
  transfers between devices with their start and end apart: 4, of which 4 were waited for; matrix products, arithmetic and copies ran while one was open for 2% of the time, Pallas kernels for 0%

commit v1 on v0

--- a/solution.py
+++ b/solution.py
@@ -1,6 +1,10 @@
+import functools
+
 import jax
 import jax.numpy as jnp
 from jax import lax
+from jax.experimental import pallas as pl
+from jax.experimental.pallas import tpu as pltpu
 from jax.sharding import PartitionSpec as P
 
 EPS = 1e-06
@@ -36,7 +40,7 @@
     return (normed * jax.nn.silu(gate_vals), new_state)
 
 
-def shards(
+def shards_plain(
     tokens,
     first_norm_gain,
     first_gate_weight,
@@ -156,6 +160,284 @@
     return (layer_out, new_state)
 
 
+MESH = pl.DeviceIdType.MESH
+BF16 = jnp.bfloat16
+F32 = jnp.float32
+
+
+def dot32(a, b):
+    return jnp.dot(a, b, preferred_element_type=F32)
+
+
+def silu(x):
+    return x * jax.nn.sigmoid(x)
+
+
+def layer_kernel(nkv, ntp, *refs):
+    (tok_h, gain1_h, wg1_h, wu1_h, wd1_h, mgain_h, wq_h, wk_h, wv_h, wo_h, ws_h, wdec_h,
+     hlog_h, bias_h, extra_h, hgain_h, state_h, wout_h, gain2_h, wg2_h, wu2_h, wd2_h,
+     out_h, new_h,
+     gain1, wg1, wu1, wd1, mgain, wq, wk, wv, wo, ws, wdec, hlog, bias, extra, hgain,
+     state, wout, gain2, wg2, wu2, wd2,
+     gath1, gath2, gath3, part1, recv1, part2, recv2, projs, projr, heads_g, halves, halfr,
+     gates_v, ks_v, qs_v, newst, out_v, load_sem, out_sem, send_sem, recv_sem) = refs
+    n = nkv * ntp
+    kv = lax.axis_index("kv")
+    tp = lax.axis_index("tp")
+    me = kv * ntp + tp
+    rows, cols = tok_h.shape
+    seqs, heads, hd, _ = state_h.shape
+    width = heads * hd
+    model = n * cols
+
+    tok_copy = pltpu.make_async_copy(tok_h, gath1.at[me], load_sem.at[0])
+    tok_copy.start()
+    order = [(gain1_h, gain1), (wg1_h, wg1), (wu1_h, wu1), (wd1_h, wd1), (mgain_h, mgain),
+             (wq_h, wq), (wk_h, wk), (wv_h, wv), (wo_h, wo), (ws_h, ws), (wdec_h, wdec),
+             (hlog_h, hlog), (bias_h, bias), (extra_h, extra), (hgain_h, hgain),
+             (state_h, state), (wout_h, wout), (gain2_h, gain2), (wg2_h, wg2),
+             (wu2_h, wu2), (wd2_h, wd2)]
+    loads = {}
+    for at, (source, dest) in enumerate(order):
+        copy = pltpu.make_async_copy(source, dest, load_sem.at[at + 1])
+        copy.start()
+        loads[id(dest)] = copy
+
+    def need(*dests):
+        for dest in dests:
+            loads[id(dest)].wait()
+
+    def peer(step):
+        to_kv = lax.rem(kv + step // ntp, nkv)
+        to_tp = lax.rem(tp + step % ntp, ntp)
+        return to_kv * ntp + to_tp, {"kv": to_kv, "tp": to_tp}
+
+    def origin(step):
+        return lax.rem(kv + nkv - step // ntp, nkv) * ntp + lax.rem(tp + ntp - step % ntp, ntp)
+
+    barrier = pltpu.get_barrier_semaphore()
+    for step in range(1, n):
+        pl.semaphore_signal(barrier, inc=1, device_id=peer(step)[1], device_id_type=MESH)
+    pl.semaphore_wait(barrier, n - 1)
+
+    def send(source, dest, phase, step):
+        copy = pltpu.make_async_remote_copy(
+            src_ref=source, dst_ref=dest, send_sem=send_sem.at[phase, step],
+            recv_sem=recv_sem.at[phase, step], device_id=peer(step)[1], device_id_type=MESH)
+        copy.start()
+        return copy
+
+    def spread(gath, phase):
+        return {step: send(gath.at[me], gath.at[me], phase, step) for step in range(1, n)}
+
+    def block_of(at):
+        return pl.ds(pl.multiple_of(at * cols, cols), cols)
+
+    def half_block(gath, copies, gain, w_gate, w_up, w_down, part, recv, phase):
+        def take(source, carry):
+            squares, gate, up = carry
+            block = gath[source].astype(F32)
+            squares = squares + jnp.sum(block * block, axis=1, keepdims=True)
+            scaled = (block * gain[:, block_of(source)]).astype(BF16)
+            gate = gate + dot32(scaled, w_gate[block_of(source), :])
+            up = up + dot32(scaled, w_up[block_of(source), :])
+            return (squares, gate, up)
+
+        hidden_cols = w_gate.shape[1]
+        need(gain, w_gate, w_up)
+        zeros = jnp.zeros((rows, hidden_cols), F32)
+        carry = take(me, (jnp.zeros((rows, 1), F32), zeros, zeros))
+        for step in range(1, n):
+            copies[step].wait()
+            carry = take(origin(step), carry)
+        squares, gate, up = carry
+        factor = lax.rsqrt(squares / model + EPS)
+        hidden = (silu(gate * factor) * (up * factor)).astype(BF16)
+        need(w_down)
+        sends = {}
+        for step in range(1, n):
+            part[step - 1] = dot32(hidden, w_down[:, block_of(peer(step)[0])]).astype(BF16)
+            sends[step] = send(part.at[step - 1], recv.at[step - 1], phase, step)
+        total = dot32(hidden, w_down[:, block_of(me)])
+        for step in range(1, n):
+            sends[step].wait()
+            total = total + recv[step - 1].astype(F32)
+        return total
+
+    tok_copy.wait()
+    copies = spread(gath1, 0)
+    share = half_block(gath1, copies, gain1, wg1, wu1, wd1, part1, recv1, 1)
+    first = (gath1[me].astype(F32) + 0.5 * share).astype(BF16)
+    gath2[me] = first
+    copies = spread(gath2, 2)
+
+    def scaled_block(source):
+        return (gath2[source].astype(F32) * mgain[:, block_of(source)]).astype(BF16)
+
+    need(mgain, wq, wk, wv, wo)
+    acc = [jnp.zeros((rows, width), F32) for _ in range(4)]
+    for step in range(ntp):
+        if step:
+            copies[step].wait()
+        source = origin(step)
+        local = block_of(lax.rem(source, ntp))
+        scaled = scaled_block(source)
+        acc = [a + dot32(scaled, w[local, :]) for a, w in zip(acc, (wq, wk, wv, wo))]
+    for role in range(4):
+        projs[:, :, role * width:(role + 1) * width] = acc[role].reshape(nkv, seqs, width).astype(BF16)
+    psends = {}
+    for dk in range(1, nkv):
+        to_kv = lax.rem(kv + dk, nkv)
+        psends[dk] = send(projs.at[to_kv], projr.at[dk - 1], 3, dk * ntp)
+
+    need(ws, wdec, hlog, bias, extra, hgain)
+    squares = jnp.zeros((rows, 1), F32)
+    beta_all = jnp.zeros((rows, ws.shape[1]), F32)
+    dec_all = jnp.zeros((rows, ws.shape[1]), F32)
+    for step in range(n):
+        if step >= ntp:
+            copies[step].wait()
+        source = origin(step)
+        block = gath2[source].astype(F32)
+        squares = squares + jnp.sum(block * block, axis=1, keepdims=True)
+        scaled = scaled_block(source)
+        beta_all = beta_all + dot32(scaled, ws[block_of(source), :])
+        dec_all = dec_all + dot32(scaled, wdec[block_of(source), :])
+    gates_v[0] = jnp.broadcast_to(lax.rsqrt(squares / model + EPS), (rows, 128))
+    gates_v[1, :, 0:ws.shape[1]] = beta_all
+    gates_v[2, :, 0:ws.shape[1]] = dec_all
+    own = pl.ds(pl.multiple_of(kv * seqs, seqs), seqs)
+    factor = gates_v[0, own, :][:, 0:1]
+
+    def own_heads(values):
+        picked = values[:, 0:heads]
+        for at in range(1, ntp):
+            picked = jnp.where(tp == at, values[:, at * heads:(at + 1) * heads], picked)
+        return picked
+
+    beta = jax.nn.sigmoid(own_heads(gates_v[1, own, :]) * factor)
+    logits = own_heads(gates_v[2, own, :]) * factor + own_heads(bias[...])
+    softplus = jnp.maximum(logits, 0.0) + jnp.log1p(jnp.exp(-jnp.abs(logits)))
+    decay = jnp.exp(extra[...] - jnp.exp(own_heads(hlog[...])) * softplus)
+
+    summed = projs[kv].astype(F32)
+    for dk in range(1, nkv):
+        psends[dk].wait()
+        summed = summed + projr[dk - 1].astype(F32)
+    summed = summed * factor
+
+    def role_head(role, h):
+        start = role * width + h * hd
+        return summed[:, start:start + hd]
+
+    def unit(u):
+        return u * lax.rsqrt(jnp.sum(u * u, axis=-1, keepdims=True) + EPS)
+
+    key_h = [unit(silu(role_head(1, h))) for h in range(heads)]
+    query_hs = [unit(silu(role_head(0, h))) * hd ** (-0.5) for h in range(heads)]
+    pad = jnp.zeros((hd - 2 * heads * seqs, hd), F32)
+    turned = jnp.concatenate(key_h + query_hs + [pad], axis=0).T
+    need(state)
+    for h in range(heads):
+        for s in range(seqs):
+            mat = state[s, h]
+            at = h * seqs + s
+            ks_v[h, s:s + 1, :] = jnp.sum(turned[:, at:at + 1] * mat, axis=0, keepdims=True)
+            at = at + heads * seqs
+            qs_v[h, s:s + 1, :] = jnp.sum(turned[:, at:at + 1] * mat, axis=0, keepdims=True)
+    corrections = []
+    decays = []
+    outs = []
+    for h in range(heads):
+        rate = jnp.broadcast_to(decay[:, h:h + 1], (seqs, hd))
+        correction = beta[:, h:h + 1] * (silu(role_head(2, h)) - rate * ks_v[h])
+        mix = jnp.sum(query_hs[h] * key_h[h], axis=1, keepdims=True)
+        read = rate * qs_v[h] + mix * correction
+        normed = read * lax.rsqrt(jnp.mean(read * read, axis=-1, keepdims=True) + EPS) * hgain[...]
+        outs.append((normed * silu(role_head(3, h))).astype(BF16))
+        corrections.append(correction)
+        decays.append(rate)
+    for h in range(heads):
+        heads_g[kv, :, h * hd:(h + 1) * hd] = outs[h]
+    hsends = {dk: send(heads_g.at[kv], heads_g.at[kv], 4, dk * ntp) for dk in range(1, nkv)}
+
+    for h in range(heads):
+        ks_v[h] = corrections[h]
+        qs_v[h] = decays[h]
+    for h in range(heads):
+        for s in range(seqs):
+            at = h * seqs + s
+            newst[s, h] = qs_v[h, s:s + 1, :] * state[s, h] + turned[:, at:at + 1] * ks_v[h, s:s + 1, :]
+    state_copy = pltpu.make_async_copy(newst, new_h, out_sem.at[0])
+    state_copy.start()
+
+    need(wout)
+    for dk in range(1, nkv):
+        hsends[dk].wait()
+    all_heads = heads_g[...].astype(F32).reshape(rows, width).astype(BF16)
+    tsends = {}
+    for step in range(1, ntp):
+        to_tp = lax.rem(tp + step, ntp)
+        halves[step - 1] = dot32(all_heads, wout[:, block_of(to_tp)]).astype(BF16)
+        tsends[step] = send(halves.at[step - 1], halfr.at[step - 1], 5, step)
+    mixed = dot32(all_heads, wout[:, block_of(tp)]).astype(BF16).astype(F32)
+    for step in range(1, ntp):
+        tsends[step].wait()
+        mixed = mixed + halfr[step - 1].astype(F32)
+    gath3[me] = (gath2[me].astype(F32) + mixed).astype(BF16)
+    copies = spread(gath3, 6)
+    last = half_block(gath3, copies, gain2, wg2, wu2, wd2, part2, recv2, 7)
+    out_v[...] = (gath3[me].astype(F32) + 0.5 * last).astype(BF16)
+    out_copy = pltpu.make_async_copy(out_v, out_h, out_sem.at[1])
+    out_copy.start()
+    out_copy.wait()
+    state_copy.wait()
+
+
+def shards(*args):
+    nkv, ntp = lax.axis_size("kv"), lax.axis_size("tp")
+    n = nkv * ntp
+    tokens, state, strength = args[0], args[16], args[10]
+    rows, cols = tokens.shape
+    seqs, heads, hd, _ = state.shape
+    if cols % 128 or ntp < 2 or nkv < 2 or 2 * seqs * heads > hd or seqs % 8:
+        return shards_plain(*args)
+    args = [a.reshape(1, -1) if a.ndim == 1 else a for a in args]
+    width = heads * hd
+    buffers = [pltpu.VMEM(a.shape, a.dtype) for a in args[1:]]
+    buffers += [pltpu.VMEM((n, rows, cols), BF16)] * 3
+    buffers += [pltpu.VMEM((n - 1, rows, cols), BF16)] * 4
+    buffers += [
+        pltpu.VMEM((nkv, seqs, 4 * width), BF16),
+        pltpu.VMEM((nkv - 1, seqs, 4 * width), BF16),
+        pltpu.VMEM((nkv, seqs, width), BF16),
+        pltpu.VMEM((ntp - 1, rows, cols), BF16),
+        pltpu.VMEM((ntp - 1, rows, cols), BF16),
+        pltpu.VMEM((3, rows, 128), F32),
+        pltpu.VMEM((heads, seqs, hd), F32),
+        pltpu.VMEM((heads, seqs, hd), F32),
+        pltpu.VMEM(state.shape, F32),
+        pltpu.VMEM((rows, cols), BF16),
+        pltpu.SemaphoreType.DMA((len(args),)),
+        pltpu.SemaphoreType.DMA((2,)),
+        pltpu.SemaphoreType.DMA((8, n)),
+        pltpu.SemaphoreType.DMA((8, n)),
+    ]
+    return pl.pallas_call(
+        functools.partial(layer_kernel, nkv, ntp),
+        out_shape=(
+            jax.ShapeDtypeStruct(tokens.shape, tokens.dtype),
+            jax.ShapeDtypeStruct(state.shape, state.dtype),
+        ),
+        in_specs=[pl.BlockSpec(memory_space=pl.ANY)] * len(args),
+        out_specs=[pl.BlockSpec(memory_space=pl.ANY)] * 2,
+        scratch_shapes=buffers,
+        compiler_params=pltpu.CompilerParams(
+            collective_id=0, has_side_effects=True, vmem_limit_bytes=60 * 1024 * 1024
+        ),
+    )(*args)
+
+
 def solution(mesh):
     placed = (
         P("dp", ("kv", "tp")),

time: 182 us -> 67 us (0.37)
  waiting for transfers between devices: 69.1 us -> 0 us
  blocking collectives: 59.7 us -> 0 us
  Pallas kernels: 0 us -> 41.4 us
  matrix products: 27.2 us -> 0 us
  local copies, waits for them, and re-layouts: 5.02 us -> 24.6 us
  between operations: 13.9 us -> 0.64 us
  other arithmetic: 6.18 us -> 0 us
    reduce_scatter x4 -> x0, waiting for transfers between devices: 69 us -> none  [the longest x1 31.5 us: shards(): lax.psum_scatter(last_terms.astype(jnp.bfloat16), ('kv', 'tp'), scatter_d...]
    all_gather x4 -> x0, blocking collectives: 45.3 us -> none  [the longest x1 16.1 us: shards(): rows_all = lax.all_gather(tokens, ('kv', 'tp'), axis=1, tiled=True)]
    pallas_call x0 -> x1, Pallas kernels: none -> 41.4 us  [shards(): pl.pallas_call(functools.partial(layer_kernel, nkv, ntp), out_shape=(jax....]
    dot_general x13 -> x0, matrix products: 27.2 us -> none  [the longest x2 9.45 us: block_terms(): return jnp.dot(hidden, w_down, preferred_element_type=jnp.float32)]
    unnamed x20 -> x13, local copies, waits for them, and re-layouts: 1.87 us -> 24.6 us
    psum x1 -> x0, blocking collectives: 14.4 us -> none  [shards(): lax.psum((jnp.sum(first32 * first32, axis=1), jnp.dot(own_scaled, beta_ro...]
    dynamic_slice x4 -> x0, local copies, waits for them, and re-layouts: 2.33 us -> none  [the longest x1 0.76 us: shards(): lax.dynamic_slice_in_dim(mixer_norm_gain, own_block * columns, columns)]
    convert_element_type x3 -> x0, other arithmetic: 2.13 us -> none  [the longest x1 1.33 us: shards(): (second_rows.astype(jnp.float32) + 0.5 * last_sum).astype(jnp.bfloat16)]
  transfers between devices with their start and end apart: 4 -> 0, of which waited for: 4 -> 0; matrix products, arithmetic and copies ran while one was open for 2% -> 0% of each run, Pallas kernels for 0% -> 0%
where the time goes in v1:
time: 67 us; the launch traced here: 66.6 us
  Pallas kernels  41.4 us (62%)
  local copies, waits for them, and re-layouts  24.6 us (37%)
    pallas_call x1, Pallas kernels, shards(): pl.pallas_call(functools.partial(layer_kernel, nkv, ntp), out_shape=(jax....  41.4 us
    unnamed x13, local copies, waits for them, and re-layouts  24.6 us

profile of v1, /device:TPU:0, one launch (start us, length us, event | category | flops | bytes accessed | tf_op | source)
XLA Modules:
  0.0 66.6 jit_solution(10670341286900739590)
XLA Ops:
  0.6 1.3 %copy.28.refs_14_ = f32[8,4]{1,0:T(8,128)} copy(f32[8,4]{0,1:T(4,128)} %param.36) | data formatting | bytes 256 | tf_op args[14]
  2.0 1.8 %copy.26.refs_10_ = bf16[2048,8]{1,0:T(8,128)(2,1)} copy(bf16[2048,8]{0,1:T(8,128)(2,1)} %param.32) | data formatting | bytes 65536 | tf_op args[10]
  3.7 1.8 %copy.27.refs_11_ = bf16[2048,8]{1,0:T(8,128)(2,1)} copy(bf16[2048,8]{0,1:T(8,128)(2,1)} %param.33) | data formatting | bytes 65536 | tf_op args[11]
  5.5 0.0 copy-start
  5.5 4.8 %copy.24.refs_2_ = bf16[2048,704]{1,0:T(8,128)(2,1)} copy(bf16[2048,704]{0,1:T(8,128)(2,1)} %param.24) | data formatting | bytes 5767168 | tf_op args[2]
  10.3 0.0 copy-done
  10.3 2.8 %copy.25.refs_3_ = bf16[2048,704]{1,0:T(8,128)(2,1)} copy(bf16[2048,704]{0,1:T(8,128)(2,1)S(1)} %copy-done) | data formatting | bytes 5767168 | tf_op args[3]
  13.1 0.0 copy-start.1
  13.1 4.8 %copy.29.refs_19_ = bf16[2048,704]{1,0:T(8,128)(2,1)} copy(bf16[2048,704]{0,1:T(8,128)(2,1)} %param.41) | data formatting | bytes 5767168 | tf_op args[19]
  17.9 0.0 copy-done.1
  17.9 2.8 %copy.30.refs_20_ = bf16[2048,704]{1,0:T(8,128)(2,1)} copy(bf16[2048,704]{0,1:T(8,128)(2,1)S(1)} %copy-done.1) | data formatting | bytes 5767168 | tf_op args[20]
  20.7 41.4 %shard_map.221 = (bf16[32,256]{1,0:T(8,128)(2,1)}, f32[8,4,128,128]{3,2,1,0:T(8,128)}) custom-call(bf16[32,256]{1,0:T(8,128)(2,1)} %refs_0_.1, f32[1,2048]{1,0:T(1,128)} %bitcast.6, bf16[2048,704]{1,0:T(8,128)(2,1)} %copy.24.refs_2_, bf16[2048,704]{1,0:T(8,128)(2,1)} %copy.25.refs_3_, bf16[704,2048]{1,0:T(8,128)(2,1)} %refs_4_.1, f32[1,2048]{1,0:T(1,128)} %bitcast.7, ...), custom_call_target="tpu_custom_call" | custom-call | tf_op jit(solution)/shard_map/pallas_call | solution.py:426
  62.1 1.3 %copy.33 = bf16[32,256]{1,0:T(8,128)(2,1)} copy(bf16[32,256]{1,0:T(8,128)(2,1)} %get-tuple-element.4) | data formatting | bytes 32768
  63.4 3.1 %copy.34 = f32[8,4,128,128]{3,2,1,0:T(8,128)} copy(f32[8,4,128,128]{3,2,1,0:T(8,128)} %get-tuple-element.5) | data formatting | bytes 4194304
Async XLA Ops:
  5.5 4.8 %copy-start = (bf16[2048,704]{0,1:T(8,128)(2,1)S(1)}, bf16[2048,704]{0,1:T(8,128)(2,1)}, u32[]{:S(2)}) copy-start(bf16[2048,704]{0,1:T(8,128)(2,1)} %param.25) | copy-start | bytes 8650756
  13.1 4.8 %copy-start.1 = (bf16[2048,704]{0,1:T(8,128)(2,1)S(1)}, bf16[2048,704]{0,1:T(8,128)(2,1)}, u32[]{:S(2)}) copy-start(bf16[2048,704]{0,1:T(8,128)(2,1)} %param.42) | copy-start | bytes 8650756

commit v2 on v1

--- a/solution.py
+++ b/solution.py
@@ -169,6 +169,10 @@
     return jnp.dot(a, b, preferred_element_type=F32)
 
 
+def dot32t(a, b):
+    return lax.dot_general(a, b, (((1,), (1,)), ((), ())), preferred_element_type=F32)
+
+
 def silu(x):
     return x * jax.nn.sigmoid(x)
 
@@ -180,7 +184,7 @@
      gain1, wg1, wu1, wd1, mgain, wq, wk, wv, wo, ws, wdec, hlog, bias, extra, hgain,
      state, wout, gain2, wg2, wu2, wd2,
      gath1, gath2, gath3, part1, recv1, part2, recv2, projs, projr, heads_g, halves, halfr,
-     gates_v, ks_v, qs_v, newst, out_v, load_sem, out_sem, send_sem, recv_sem) = refs
+     stat, statr, split, ks_v, qs_v, newst, out_v, load_sem, out_sem, send_sem, recv_sem) = refs
     n = nkv * ntp
     kv = lax.axis_index("kv")
     tp = lax.axis_index("tp")
@@ -198,10 +202,15 @@
              (state_h, state), (wout_h, wout), (gain2_h, gain2), (wg2_h, wg2),
              (wu2_h, wu2), (wd2_h, wd2)]
     loads = {}
-    for at, (source, dest) in enumerate(order):
-        copy = pltpu.make_async_copy(source, dest, load_sem.at[at + 1])
-        copy.start()
-        loads[id(dest)] = copy
+
+    def fetch(start, stop):
+        for at in range(start, stop):
+            source, dest = order[at]
+            copy = pltpu.make_async_copy(source, dest, load_sem.at[at + 1])
+            copy.start()
+            loads[id(dest)] = copy
+
+    fetch(0, 4)
 
     def need(*dests):
         for dest in dests:
@@ -227,24 +236,25 @@
         copy.start()
         return copy
 
-    def spread(gath, phase):
-        return {step: send(gath.at[me], gath.at[me], phase, step) for step in range(1, n)}
+    def spread(gath, phase, stop=n):
+        return {step: send(gath.at[me], gath.at[me], phase, step) for step in range(1, stop)}
 
     def block_of(at):
         return pl.ds(pl.multiple_of(at * cols, cols), cols)
 
-    def half_block(gath, copies, gain, w_gate, w_up, w_down, part, recv, phase):
+    def half_block(gath, copies, gain, w_gate, w_up, w_down, part, recv, phase, then):
         def take(source, carry):
             squares, gate, up = carry
             block = gath[source].astype(F32)
             squares = squares + jnp.sum(block * block, axis=1, keepdims=True)
             scaled = (block * gain[:, block_of(source)]).astype(BF16)
-            gate = gate + dot32(scaled, w_gate[block_of(source), :])
-            up = up + dot32(scaled, w_up[block_of(source), :])
+            gate = gate + dot32t(scaled, w_gate[:, block_of(source)])
+            up = up + dot32t(scaled, w_up[:, block_of(source)])
             return (squares, gate, up)
 
-        hidden_cols = w_gate.shape[1]
+        hidden_cols = w_gate.shape[0]
         need(gain, w_gate, w_up)
+        fetch(*then)
         zeros = jnp.zeros((rows, hidden_cols), F32)
         carry = take(me, (jnp.zeros((rows, 1), F32), zeros, zeros))
         for step in range(1, n):
@@ -266,15 +276,32 @@
 
     tok_copy.wait()
     copies = spread(gath1, 0)
-    share = half_block(gath1, copies, gain1, wg1, wu1, wd1, part1, recv1, 1)
+    share = half_block(gath1, copies, gain1, wg1, wu1, wd1, part1, recv1, 1, (4, 17))
     first = (gath1[me].astype(F32) + 0.5 * share).astype(BF16)
     gath2[me] = first
-    copies = spread(gath2, 2)
+    copies = spread(gath2, 2, ntp)
+    fetch(17, len(order))
 
     def scaled_block(source):
         return (gath2[source].astype(F32) * mgain[:, block_of(source)]).astype(BF16)
 
-    need(mgain, wq, wk, wv, wo)
+    need(mgain, ws, wdec, hlog, bias, extra, hgain)
+    all_heads = ws.shape[0]
+    first32 = first.astype(F32)
+    scaled = scaled_block(me)
+    stat[...] = jnp.zeros_like(stat)
+    for at, values in (
+        (0, dot32t(scaled, ws[:, block_of(me)])),
+        (all_heads, dot32t(scaled, wdec[:, block_of(me)])),
+        (2 * all_heads, jnp.sum(first32 * first32, axis=1, keepdims=True)),
+    ):
+        lanes = values.shape[1]
+        stat[:, :, at:at + lanes] = values.reshape(nkv, seqs, lanes)
+    ssends = {}
+    for step in range(1, n):
+        ssends[step] = send(stat.at[peer(step)[0] // ntp], statr.at[step - 1], 8, step)
+
+    need(wq, wk, wv, wo)
     acc = [jnp.zeros((rows, width), F32) for _ in range(4)]
     for step in range(ntp):
         if step:
@@ -290,24 +317,20 @@
         to_kv = lax.rem(kv + dk, nkv)
         psends[dk] = send(projs.at[to_kv], projr.at[dk - 1], 3, dk * ntp)
 
-    need(ws, wdec, hlog, bias, extra, hgain)
-    squares = jnp.zeros((rows, 1), F32)
-    beta_all = jnp.zeros((rows, ws.shape[1]), F32)
-    dec_all = jnp.zeros((rows, ws.shape[1]), F32)
-    for step in range(n):
-        if step >= ntp:
-            copies[step].wait()
-        source = origin(step)
-        block = gath2[source].astype(F32)
-        squares = squares + jnp.sum(block * block, axis=1, keepdims=True)
-        scaled = scaled_block(source)
-        beta_all = beta_all + dot32(scaled, ws[block_of(source), :])
-        dec_all = dec_all + dot32(scaled, wdec[block_of(source), :])
-    gates_v[0] = jnp.broadcast_to(lax.rsqrt(squares / model + EPS), (rows, 128))
-    gates_v[1, :, 0:ws.shape[1]] = beta_all
-    gates_v[2, :, 0:ws.shape[1]] = dec_all
-    own = pl.ds(pl.multiple_of(kv * seqs, seqs), seqs)
-    factor = gates_v[0, own, :][:, 0:1]
+    need(state)
+    for h in range(heads):
+        for s in range(seqs):
+            mat = state[s, h]
+            high = mat.astype(BF16)
+            beside = slice((s % 2) * hd, (s % 2 + 1) * hd)
+            split[h, s // 2, 0:hd, beside] = high
+            split[h, s // 2, hd:2 * hd, beside] = (mat - high.astype(F32)).astype(BF16)
+
+    totals = stat[kv]
+    for step in range(1, n):
+        ssends[step].wait()
+        totals = totals + statr[step - 1]
+    factor = lax.rsqrt(totals[:, 2 * all_heads:2 * all_heads + 1] / model + EPS)
 
     def own_heads(values):
         picked = values[:, 0:heads]
@@ -315,10 +338,10 @@
             picked = jnp.where(tp == at, values[:, at * heads:(at + 1) * heads], picked)
         return picked
 
-    beta = jax.nn.sigmoid(own_heads(gates_v[1, own, :]) * factor)
-    logits = own_heads(gates_v[2, own, :]) * factor + own_heads(bias[...])
+    beta = jax.nn.sigmoid(own_heads(totals) * factor)
+    logits = own_heads(totals[:, all_heads:2 * all_heads]) * factor + own_heads(bias[...])
     softplus = jnp.maximum(logits, 0.0) + jnp.log1p(jnp.exp(-jnp.abs(logits)))
-    decay = jnp.exp(extra[...] - jnp.exp(own_heads(hlog[...])) * softplus)
+    decay = jnp.exp(extra[...].T - jnp.exp(own_heads(hlog[...])) * softplus)
 
     summed = projs[kv].astype(F32)
     for dk in range(1, nkv):
@@ -335,24 +358,33 @@
 
     key_h = [unit(silu(role_head(1, h))) for h in range(heads)]
     query_hs = [unit(silu(role_head(0, h))) * hd ** (-0.5) for h in range(heads)]
-    pad = jnp.zeros((hd - 2 * heads * seqs, hd), F32)
-    turned = jnp.concatenate(key_h + query_hs + [pad], axis=0).T
-    need(state)
+    row_at = lax.broadcasted_iota(jnp.int32, (seqs, hd), 0)
+    recalled = []
+    asked = []
     for h in range(heads):
-        for s in range(seqs):
-            mat = state[s, h]
-            at = h * seqs + s
-            ks_v[h, s:s + 1, :] = jnp.sum(turned[:, at:at + 1] * mat, axis=0, keepdims=True)
-            at = at + heads * seqs
-            qs_v[h, s:s + 1, :] = jnp.sum(turned[:, at:at + 1] * mat, axis=0, keepdims=True)
+        both = jnp.concatenate([key_h[h], query_hs[h]], axis=0)
+        high = both.astype(BF16).astype(F32)
+        terms = jnp.concatenate([high, both - high], axis=0).astype(BF16)
+        terms = jnp.concatenate([terms, terms], axis=1)
+        sums = [jnp.zeros((seqs, hd), F32)] * 2
+        for half in range(seqs // 2):
+            found = dot32(terms, split[h, half])
+            found = found[0:2 * seqs] + found[2 * seqs:4 * seqs]
+            for s in (0, 1):
+                own_row = row_at == 2 * half + s
+                for role in (0, 1):
+                    part = found[role * seqs:(role + 1) * seqs, s * hd:(s + 1) * hd]
+                    sums[role] = jnp.where(own_row, part, sums[role])
+        recalled.append(sums[0])
+        asked.append(sums[1])
     corrections = []
     decays = []
     outs = []
     for h in range(heads):
         rate = jnp.broadcast_to(decay[:, h:h + 1], (seqs, hd))
-        correction = beta[:, h:h + 1] * (silu(role_head(2, h)) - rate * ks_v[h])
+        correction = beta[:, h:h + 1] * (silu(role_head(2, h)) - rate * recalled[h])
         mix = jnp.sum(query_hs[h] * key_h[h], axis=1, keepdims=True)
-        read = rate * qs_v[h] + mix * correction
+        read = rate * asked[h] + mix * correction
         normed = read * lax.rsqrt(jnp.mean(read * read, axis=-1, keepdims=True) + EPS) * hgain[...]
         outs.append((normed * silu(role_head(3, h))).astype(BF16))
         corrections.append(correction)
@@ -361,6 +393,8 @@
         heads_g[kv, :, h * hd:(h + 1) * hd] = outs[h]
     hsends = {dk: send(heads_g.at[kv], heads_g.at[kv], 4, dk * ntp) for dk in range(1, nkv)}
 
+    pad = jnp.zeros((hd - heads * seqs, hd), F32)
+    turned = jnp.concatenate(key_h + [pad], axis=0).T
     for h in range(heads):
         ks_v[h] = corrections[h]
         qs_v[h] = decays[h]
@@ -374,19 +408,19 @@
     need(wout)
     for dk in range(1, nkv):
         hsends[dk].wait()
-    all_heads = heads_g[...].astype(F32).reshape(rows, width).astype(BF16)
+    gathered = heads_g[...].astype(F32).reshape(rows, width).astype(BF16)
     tsends = {}
     for step in range(1, ntp):
         to_tp = lax.rem(tp + step, ntp)
-        halves[step - 1] = dot32(all_heads, wout[:, block_of(to_tp)]).astype(BF16)
+        halves[step - 1] = dot32(gathered, wout[:, block_of(to_tp)]).astype(BF16)
         tsends[step] = send(halves.at[step - 1], halfr.at[step - 1], 5, step)
-    mixed = dot32(all_heads, wout[:, block_of(tp)]).astype(BF16).astype(F32)
+    mixed = dot32(gathered, wout[:, block_of(tp)]).astype(BF16).astype(F32)
     for step in range(1, ntp):
         tsends[step].wait()
         mixed = mixed + halfr[step - 1].astype(F32)
     gath3[me] = (gath2[me].astype(F32) + mixed).astype(BF16)
     copies = spread(gath3, 6)
-    last = half_block(gath3, copies, gain2, wg2, wu2, wd2, part2, recv2, 7)
+    last = half_block(gath3, copies, gain2, wg2, wu2, wd2, part2, recv2, 7, (0, 0))
     out_v[...] = (gath3[me].astype(F32) + 0.5 * last).astype(BF16)
     out_copy = pltpu.make_async_copy(out_v, out_h, out_sem.at[1])
     out_copy.start()
@@ -400,9 +434,11 @@
     tokens, state, strength = args[0], args[16], args[10]
     rows, cols = tokens.shape
     seqs, heads, hd, _ = state.shape
-    if cols % 128 or ntp < 2 or nkv < 2 or 2 * seqs * heads > hd or seqs % 8:
+    if cols % 128 or ntp < 2 or nkv < 2 or seqs * heads > hd or seqs % 8:
         return shards_plain(*args)
     args = [a.reshape(1, -1) if a.ndim == 1 else a for a in args]
+    for at in (2, 3, 10, 11, 14, 19, 20):
+        args[at] = args[at].T
     width = heads * hd
     buffers = [pltpu.VMEM(a.shape, a.dtype) for a in args[1:]]
     buffers += [pltpu.VMEM((n, rows, cols), BF16)] * 3
@@ -413,15 +449,17 @@
         pltpu.VMEM((nkv, seqs, width), BF16),
         pltpu.VMEM((ntp - 1, rows, cols), BF16),
         pltpu.VMEM((ntp - 1, rows, cols), BF16),
-        pltpu.VMEM((3, rows, 128), F32),
+        pltpu.VMEM((nkv, seqs, 128), F32),
+        pltpu.VMEM((n - 1, seqs, 128), F32),
+        pltpu.VMEM((heads, seqs // 2, 2 * hd, 2 * hd), BF16),
         pltpu.VMEM((heads, seqs, hd), F32),
         pltpu.VMEM((heads, seqs, hd), F32),
         pltpu.VMEM(state.shape, F32),
         pltpu.VMEM((rows, cols), BF16),
         pltpu.SemaphoreType.DMA((len(args),)),
         pltpu.SemaphoreType.DMA((2,)),
-        pltpu.SemaphoreType.DMA((8, n)),
-        pltpu.SemaphoreType.DMA((8, n)),
+        pltpu.SemaphoreType.DMA((9, n)),
+        pltpu.SemaphoreType.DMA((9, n)),
     ]
     return pl.pallas_call(
         functools.partial(layer_kernel, nkv, ntp),

time: 67 us -> 45.3 us (0.68)
  local copies, waits for them, and re-layouts: 24.6 us -> 4.46 us
  Pallas kernels: 41.4 us -> 39.9 us
    unnamed x13 -> x2, local copies, waits for them, and re-layouts: 24.6 us -> 4.46 us
    pallas_call x1, Pallas kernels: 41.4 us -> 39.9 us  [shards(): pl.pallas_call(functools.partial(layer_kernel, nkv, ntp), out_shape=(jax....]
where the time goes in v2:
time: 45.3 us; the launch traced here: 45 us
  Pallas kernels  39.9 us (88%)
  local copies, waits for them, and re-layouts  4.46 us (10%)
  between operations  0.65 us (1%)
    pallas_call x1, Pallas kernels, shards(): pl.pallas_call(functools.partial(layer_kernel, nkv, ntp), out_shape=(jax....  39.9 us
    unnamed x2, local copies, waits for them, and re-layouts  4.46 us

profile of v2, /device:TPU:0, one launch (start us, length us, event | category | flops | bytes accessed | tf_op | source)
XLA Modules:
  0.0 45.0 jit_solution(16262272930017383182)
XLA Ops:
  0.6 39.9 %shard_map.221 = (bf16[32,256]{1,0:T(8,128)(2,1)}, f32[8,4,128,128]{3,2,1,0:T(8,128)}) custom-call(bf16[32,256]{1,0:T(8,128)(2,1)} %refs_0_.1, f32[1,2048]{1,0:T(1,128)} %bitcast.19, bf16[704,2048]{1,0:T(8,128)(2,1)} %bitcast.13, bf16[704,2048]{1,0:T(8,128)(2,1)} %bitcast.14, bf16[704,2048]{1,0:T(8,128)(2,1)} %refs_4_.1, f32[1,2048]{1,0:T(1,128)} %bitcast.20, ...), custom_call_target="tpu_custom_call" | custom-call | tf_op jit(solution)/shard_map/pallas_call | solution.py:464
  40.5 1.3 %copy.26 = bf16[32,256]{1,0:T(8,128)(2,1)} copy(bf16[32,256]{1,0:T(8,128)(2,1)} %get-tuple-element.4) | data formatting | bytes 32768
  41.9 3.1 %copy.27 = f32[8,4,128,128]{3,2,1,0:T(8,128)} copy(f32[8,4,128,128]{3,2,1,0:T(8,128)} %get-tuple-element.5) | data formatting | bytes 4194304

commit v3 on v2

--- a/solution.py
+++ b/solution.py
@@ -428,6 +428,25 @@
     state_copy.wait()
 
 
+def hand_over(rows_h, state_h, rows_o, state_o, rows_v, state_v, in_sem, out_sem):
+    count = in_sem.shape[0] - 1
+    size = state_h.shape[0] // count
+    spans = [pl.ds(at * size, size) for at in range(count)]
+    ins = [pltpu.make_async_copy(state_h.at[span], state_v.at[span], in_sem.at[at])
+           for at, span in enumerate(spans)]
+    outs = [pltpu.make_async_copy(state_v.at[span], state_o.at[span], out_sem.at[at])
+            for at, span in enumerate(spans)]
+    ins.append(pltpu.make_async_copy(rows_h, rows_v, in_sem.at[count]))
+    outs.append(pltpu.make_async_copy(rows_v, rows_o, out_sem.at[count]))
+    for copy in ins:
+        copy.start()
+    for arrived, copy in zip(ins, outs):
+        arrived.wait()
+        copy.start()
+    for copy in outs:
+        copy.wait()
+
+
 def shards(*args):
     nkv, ntp = lax.axis_size("kv"), lax.axis_size("tp")
     n = nkv * ntp
@@ -461,7 +480,7 @@
         pltpu.SemaphoreType.DMA((9, n)),
         pltpu.SemaphoreType.DMA((9, n)),
     ]
-    return pl.pallas_call(
+    results = pl.pallas_call(
         functools.partial(layer_kernel, nkv, ntp),
         out_shape=(
             jax.ShapeDtypeStruct(tokens.shape, tokens.dtype),
@@ -474,6 +493,23 @@
             collective_id=0, has_side_effects=True, vmem_limit_bytes=60 * 1024 * 1024
         ),
     )(*args)
+    pieces = 8 if seqs % 8 == 0 else 1
+    return pl.pallas_call(
+        hand_over,
+        out_shape=(
+            jax.ShapeDtypeStruct(tokens.shape, tokens.dtype),
+            jax.ShapeDtypeStruct(state.shape, state.dtype),
+        ),
+        in_specs=[pl.BlockSpec(memory_space=pl.ANY)] * 2,
+        out_specs=[pl.BlockSpec(memory_space=pl.ANY)] * 2,
+        scratch_shapes=[
+            pltpu.VMEM(tokens.shape, tokens.dtype),
+            pltpu.VMEM(state.shape, state.dtype),
+            pltpu.SemaphoreType.DMA((pieces + 1,)),
+            pltpu.SemaphoreType.DMA((pieces + 1,)),
+        ],
+        compiler_params=pltpu.CompilerParams(vmem_limit_bytes=60 * 1024 * 1024),
+    )(*results)
 
 
 def solution(mesh):

time: 45.3 us -> 43.1 us (0.951)
  local copies, waits for them, and re-layouts: 4.46 us -> 0 us
  Pallas kernels: 39.9 us -> 42.3 us
    unnamed x2 -> x0, local copies, waits for them, and re-layouts: 4.46 us -> none
    pallas_call x0 -> x1, Pallas kernels: none -> 2.41 us  [shards(): pl.pallas_call(hand_over, out_shape=(jax.ShapeDtypeStruct(tokens.shape, t...]
where the time goes in v3:
time: 43.1 us; the launch traced here: 43 us
  Pallas kernels  42.3 us (98%)
  between operations  0.65 us (2%)
    pallas_call x1, Pallas kernels, shards(): pl.pallas_call(functools.partial(layer_kernel, nkv, ntp), out_shape=(jax....  39.9 us
    pallas_call x1, Pallas kernels, shards(): pl.pallas_call(hand_over, out_shape=(jax.ShapeDtypeStruct(tokens.shape, t...  2.41 us

profile of v3, /device:TPU:0, one launch (start us, length us, event | category | flops | bytes accessed | tf_op | source)
XLA Modules:
  0.0 43.0 jit_solution(12454482877433316743)
XLA Ops:
  0.6 39.9 %shard_map.221 = (bf16[32,256]{1,0:T(8,128)(2,1)}, f32[8,4,128,128]{3,2,1,0:T(8,128)}) custom-call(bf16[32,256]{1,0:T(8,128)(2,1)} %refs_0_.1, f32[1,2048]{1,0:T(1,128)} %bitcast.19, bf16[704,2048]{1,0:T(8,128)(2,1)} %bitcast.13, bf16[704,2048]{1,0:T(8,128)(2,1)} %bitcast.14, bf16[704,2048]{1,0:T(8,128)(2,1)} %refs_4_.1, f32[1,2048]{1,0:T(1,128)} %bitcast.20, ...), custom_call_target="tpu_custom_call" | custom-call | tf_op jit(solution)/shard_map/pallas_call | solution.py:483
  40.5 2.4 %shard_map.222 = (bf16[32,256]{1,0:T(8,128)(2,1)}, f32[8,4,128,128]{3,2,1,0:T(8,128)}) custom-call(bf16[32,256]{1,0:T(8,128)(2,1)} %get-tuple-element.4.rows_h, f32[8,4,128,128]{3,2,1,0:T(8,128)} %get-tuple-element.5.state_h), custom_call_target="tpu_custom_call" | custom-call | tf_op jit(solution)/shard_map/pallas_call | solution.py:497
